TPU v7x, 32 devices: a whole 2x2x4 slice. The times are simulated.
32 devices in a mesh: grp: 2 (over y), ra: 4 (over z), cb: 4 (over x, core).
Axes of the slice: x: 2, y: 2, z: 4, core: 2. Of those that a mesh axis runs over, the one named last changes fastest.
Arguments:
- stream: bfloat16 [256, 4096], P('grp', 'ra'), parts along dimension 0, may hold values from -180 to 180
- w_gate: float32 [2, 4096, 11264], P(None, 'ra', 'cb'), may hold values from -0.09375 to 0.09375
- w_up: float32 [2, 4096, 11264], P(None, 'ra', 'cb'), may hold values from -0.09375 to 0.09375
- w_down: float32 [2, 11264, 4096], P(None, 'cb', 'ra'), may hold values from -0.0546875 to 0.0546875
- gate_scale: float32 [2, 11264], P(None, 'cb'), may hold values from 0.5 to 2
- up_scale: float32 [2, 11264], P(None, 'cb'), may hold values from 0.5 to 2
- down_scale: float32 [2, 4096], P(None, 'ra'), may hold values from 0.5 to 2
- pre_gain: float32 [2, 4096], P(None, 'ra'), may hold values from 0.1 to 1.9
- out_gain: float32 [4096], P('ra'), may hold values from 0.1 to 1.9
Outputs:
- normed: bfloat16 [256, 4096], P('grp', 'ra'), parts along dimension 0
There are 2 independent parts, one for each index of `grp`. A program takes and returns all parts, laid end to end along the dimension named above; an argument that names none is the same for every part. Nothing has to cross between parts.
All inputs are finite; a program needn't handle non-finite values.
Results may differ from a plain program's by a relative error of at most 0.018.
Values may be sent and summed in bfloat16 or wider, within the bound.
A program may use at most 192 MiB of HBM per device.

v0:
```python
import jax
import jax.numpy as jnp
from jax import lax
from jax.sharding import PartitionSpec as P

D = 4096
LAYERS = 2


def local(stream, w_gate, w_up, w_down, gate_scale, up_scale, down_scale, pre_gain, out_gain):
    current = stream
    tokens = stream.shape[0]
    share = tokens // lax.axis_size("ra")
    for layer in range(LAYERS):
        xvals = current.astype(jnp.float32)
        squares = jnp.sum(xvals * xvals, axis=1)
        scaled = (xvals * pre_gain[layer]).astype(jnp.bfloat16)
        gate_part = jnp.dot(
            scaled, w_gate[layer].astype(jnp.bfloat16), preferred_element_type=jnp.float32
        )
        up_part = jnp.dot(
            scaled, w_up[layer].astype(jnp.bfloat16), preferred_element_type=jnp.float32
        )
        down_local = w_down[layer].astype(jnp.bfloat16)
        total = lax.psum(squares, "ra")
        operands = (gate_part, up_part)
        summed = (
            lax.psum_scatter(operands[0], "ra", scatter_dimension=0, tiled=True),
            lax.psum_scatter(operands[1], "ra", scatter_dimension=0, tiled=True),
        )
        own_rows = lax.dynamic_slice_in_dim(total, lax.axis_index("ra") * share, share)
        rinv = lax.rsqrt(own_rows / D + 1e-06)[:, None]
        gate = summed[0] * rinv * gate_scale[layer]
        upper = summed[1] * rinv * up_scale[layer]
        hidden = (jax.nn.silu(gate) * upper).astype(jnp.bfloat16)
        terms = jnp.dot(
            lax.all_gather(hidden, "ra", axis=0, tiled=True),
            down_local,
            preferred_element_type=jnp.float32,
        )
        branch = lax.psum(terms.astype(jnp.bfloat16), "cb").astype(jnp.float32) * down_scale[layer]
        current = (0.5 * xvals + branch).astype(jnp.bfloat16)
    xvals = current.astype(jnp.float32)
    final_sum = lax.psum(jnp.sum(xvals * xvals, axis=1), "ra")
    rinv = lax.rsqrt(final_sum / D + 1e-06)[:, None]
    return (xvals * rinv * out_gain).astype(jnp.bfloat16)


def solution(mesh):
    placed = (
        P("grp", "ra"),
        P(None, "ra", "cb"),
        P(None, "ra", "cb"),
        P(None, "cb", "ra"),
        P(None, "cb"),
        P(None, "cb"),
        P(None, "ra"),
        P(None, "ra"),
        P("ra"),
    )
    return jax.shard_map(
        local, mesh=mesh, in_specs=placed, out_specs=P("grp", "ra"), check_vma=False
    )
```

profile of v0, /device:TPU:0, one launch (start us, length us, event | category | flops | bytes accessed | tf_op | source)
XLA Modules:
  0.0 296.9 jit_solution(10310652706290276706)
XLA Ops:
  6.5 0.8 fusion.24
  7.3 0.0 copy-start.2
  7.3 8.6 %convert.12 = bf16[2,1024,2816]{2,1,0:T(8,128)(2,1)S(1)} convert(f32[2,1024,2816]{2,1,0:T(8,128)} %param.10) | non-fusion elementwise | flops 5767168 | bytes 34603008 | tf_op jit(solution)/shard_map/convert.5
  15.9 4.2 %copy-done.1 = bf16[2,1024,2816]{2,1,0:T(8,128)(2,1)} copy-done((bf16[2,1024,2816]{2,1,0:T(8,128)(2,1)}, bf16[2,1024,2816]{2,1,0:T(8,128)(2,1)S(1)}, u32[]{:S(2)}) %copy-start.1) | copy-done | bytes 11534360
  20.1 0.0 copy-done.2
  20.1 2.0 fusion.5
  22.2 0.0 reduce-scatter.5.cloned.1.call-update
  22.2 0.0 reduce-scatter.7.cloned.1.call-start
  22.2 8.6 %convert.13 = bf16[2,1024,2816]{2,1,0:T(8,128)(2,1)S(1)} convert(f32[2,1024,2816]{2,1,0:T(8,128)} %param.11) | non-fusion elementwise | flops 5767168 | bytes 34603008 | tf_op jit(solution)/shard_map/convert.4
  30.8 4.2 %copy-done = bf16[2,1024,2816]{2,1,0:T(8,128)(2,1)} copy-done((bf16[2,1024,2816]{2,1,0:T(8,128)(2,1)}, bf16[2,1024,2816]{2,1,0:T(8,128)(2,1)S(1)}, u32[]{:S(2)}) %copy-start) | copy-done | bytes 11534360
  35.0 2.1 fusion.4
  37.1 0.0 reduce-scatter.7.cloned.1.call-update
  37.1 0.0 all-reduce.3.cloned.1.call-start
  37.2 0.0 copy-start.3
  37.2 0.0 copy-start.4
  37.2 12.6 %convert.14 = bf16[2,2816,1024]{2,1,0:T(8,128)(2,1)} convert(f32[2,2816,1024]{2,1,0:T(8,128)} %param.12) | non-fusion elementwise | flops 5767168 | bytes 34603008 | tf_op jit(solution)/shard_map/convert.3
  49.8 0.1 fusion.14
  50.0 13.6 %psum.35 = f32[128]{0:T(128)S(1)} all-reduce(f32[128]{0:T(128)S(1)} %fusion.14), channel_id=1, replica_groups=mesh['grp'=2,'ra'=4,'cb'=4] {'ra'}, use_global_device_ids=true, to_apply=%region_2.0 | all-reduce | flops 128 | bytes 1024 | tf_op jit(solution)/shard_map/psum | solution.py:25
  63.6 0.1 add_rsqrt_fusion.2
  63.7 0.1 slice_reduce_fusion
  63.8 0.0 reduce-scatter.5.cloned.1.call-done
  63.8 29.2 %reduce-scatter.7.cloned.1.call-done = f32[32,2816]{1,0:T(8,128)} async-done(((f32[128,2816]{1,0:T(8,128)}), f32[32,2816]{1,0:T(8,128)}) %reduce-scatter.7.cloned.1.call-update) | async-done | bytes 360464 | tf_op jit(solution)/shard_map/reduce_scatter | solution.py:29
  93.0 1.3 multiply_convert_fusion.1
  94.3 17.2 %all_gather.6 = bf16[128,2816]{1,0:T(8,128)(2,1)S(1)} all-gather(bf16[32,2816]{1,0:T(8,128)(2,1)S(1)} %multiply_convert_fusion.1), channel_id=1, replica_groups=mesh['grp'=2,'ra'=4,'cb'=4] {'ra'}, dimensions={0}, use_global_device_ids=true | all-gather | bytes 901120 | tf_op jit(solution)/shard_map/all_gather | solution.py:37
  111.5 4.3 %fusion.6 = bf16[128,1024]{1,0:T(8,128)(2,1)} fusion(bf16[128,2816]{1,0:T(8,128)(2,1)S(1)} %all_gather.6, bf16[2,2816,1024]{2,1,0:T(8,128)(2,1)} %convert.14), kind=kOutput, calls=%fused_computation.12 | convolution fusion | flops 738328576 | bytes 6750208 | tf_op jit(solution)/shard_map/dot_general | solution.py:36
  115.8 0.0 all-reduce.3.cloned.1.call-update
  115.8 0.0 reduce-scatter.9.cloned.1.call-start
  115.9 31.3 %all-reduce.3.cloned.1.call-done = bf16[128,1024]{1,0:T(8,128)(2,1)} async-done(((bf16[128,1024]{1,0:T(8,128)(2,1)}), bf16[128,1024]{1,0:T(8,128)(2,1)}) %all-reduce.3.cloned.1.call-update) | async-done | bytes 262160 | tf_op jit(solution)/shard_map/psum | solution.py:41
  147.2 1.2 fusion.18
  148.4 4.7 %fusion.2 = f32[128,2816]{1,0:T(8,128)} fusion(bf16[2,1024,2816]{2,1,0:T(8,128)(2,1)} %copy-done.1, bf16[128,1024]{1,0:T(8,128)(2,1)S(1)} %get-tuple-element.10, f32[1024]{0:T(1024)S(1)} %bitcast.31), kind=kOutput, calls=%fused_computation.5 | convolution fusion | flops 738590720 | bytes 7475200 | tf_op jit(solution)/shard_map/dot_general | solution.py:18
  153.1 0.0 reduce-scatter.9.cloned.1.call-update
  153.1 0.0 reduce-scatter.11.cloned.1.call-start
  153.1 4.7 %fusion.1 = f32[128,2816]{1,0:T(8,128)} fusion(bf16[2,1024,2816]{2,1,0:T(8,128)(2,1)} %copy-done, bf16[128,1024]{1,0:T(8,128)(2,1)S(1)} %get-tuple-element.10, f32[1024]{0:T(1024)S(1)} %bitcast.32), kind=kOutput, calls=%fused_computation.3 | convolution fusion | flops 738590720 | bytes 7475200 | tf_op jit(solution)/shard_map/dot_general | solution.py:21
  157.8 0.0 reduce-scatter.11.cloned.1.call-update
  157.8 0.0 copy-start.6
  157.9 0.0 all-reduce.5.cloned.1.call-start
  157.9 12.3 %psum.37 = f32[128]{0:T(128)S(1)} all-reduce(f32[128]{0:T(128)S(1)} %get-tuple-element.9), channel_id=1, replica_groups=mesh['grp'=2,'ra'=4,'cb'=4] {'ra'}, use_global_device_ids=true, to_apply=%region_7.8 | all-reduce | flops 128 | bytes 1024 | tf_op jit(solution)/shard_map/psum | solution.py:25
  170.2 0.1 add_rsqrt_fusion.1
  170.3 16.5 %reduce-scatter.9.cloned.1.call-done = f32[32,2816]{1,0:T(8,128)} async-done(((f32[128,2816]{1,0:T(8,128)}), f32[32,2816]{1,0:T(8,128)}) %reduce-scatter.9.cloned.1.call-update) | async-done | bytes 360464 | tf_op jit(solution)/shard_map/reduce_scatter | solution.py:28
  186.8 34.4 %reduce-scatter.11.cloned.1.call-done = f32[32,2816]{1,0:T(8,128)} async-done(((f32[128,2816]{1,0:T(8,128)}), f32[32,2816]{1,0:T(8,128)}) %reduce-scatter.11.cloned.1.call-update) | async-done | bytes 360464 | tf_op jit(solution)/shard_map/reduce_scatter | solution.py:29
  221.2 1.3 multiply_convert_fusion
  222.5 17.2 %all_gather.7 = bf16[128,2816]{1,0:T(8,128)(2,1)S(1)} all-gather(bf16[32,2816]{1,0:T(8,128)(2,1)S(1)} %multiply_convert_fusion), channel_id=1, replica_groups=mesh['grp'=2,'ra'=4,'cb'=4] {'ra'}, dimensions={0}, use_global_device_ids=true | all-gather | bytes 901120 | tf_op jit(solution)/shard_map/all_gather | solution.py:37
  239.6 4.3 %fusion.7 = bf16[128,1024]{1,0:T(8,128)(2,1)} fusion(bf16[128,2816]{1,0:T(8,128)(2,1)S(1)} %all_gather.7, bf16[2,2816,1024]{2,1,0:T(8,128)(2,1)} %convert.14), kind=kOutput, calls=%fused_computation.13 | convolution fusion | flops 738328576 | bytes 6750208 | tf_op jit(solution)/shard_map/dot_general | solution.py:36
  244.0 0.0 all-reduce.5.cloned.1.call-update
  244.0 31.5 %all-reduce.5.cloned.1.call-done = bf16[128,1024]{1,0:T(8,128)(2,1)} async-done(((bf16[128,1024]{1,0:T(8,128)(2,1)}), bf16[128,1024]{1,0:T(8,128)(2,1)}) %all-reduce.5.cloned.1.call-update) | async-done | bytes 262160 | tf_op jit(solution)/shard_map/psum | solution.py:41
  275.5 1.2 fusion.8
  276.6 11.7 %psum.39 = f32[128]{0:T(128)S(1)} all-reduce(f32[128]{0:T(128)S(1)} %fusion.8), channel_id=1, replica_groups=mesh['grp'=2,'ra'=4,'cb'=4] {'ra'}, use_global_device_ids=true, to_apply=%region_11.12 | all-reduce | flops 128 | bytes 1024 | tf_op jit(solution)/shard_map/psum | solution.py:44
  288.3 1.8 fusion.10
  (10 shorter events, 0.0 us)
Async XLA Ops:
  6.5 57.3 %reduce-scatter.5.cloned.1.call-start = ((), (), s32[]{:S(2)}) async-start(), calls=%async_computation.4 | async-start | bytes 1802240 | tf_op jit(solution)/shard_map/reduce_scatter | solution.py:28
  7.3 12.8 %copy-start.2 = (bf16[128,1024]{1,0:T(8,128)(2,1)S(1)}, bf16[128,1024]{1,0:T(8,128)(2,1)}, u32[]{:S(2)}) copy-start(bf16[128,1024]{1,0:T(8,128)(2,1)} %param.9) | copy-start | bytes 786436
  15.9 4.2 %copy-start.1 = (bf16[2,1024,2816]{2,1,0:T(8,128)(2,1)}, bf16[2,1024,2816]{2,1,0:T(8,128)(2,1)S(1)}, u32[]{:S(2)}) copy-start(bf16[2,1024,2816]{2,1,0:T(8,128)(2,1)S(1)} %convert.12) | copy-start | bytes 34603012
  22.2 70.9 %reduce-scatter.7.cloned.1.call-start = ((), (), s32[]{:S(2)}) async-start(), calls=%async_computation.5 | async-start | bytes 1802240 | tf_op jit(solution)/shard_map/reduce_scatter | solution.py:29
  30.8 4.2 %copy-start = (bf16[2,1024,2816]{2,1,0:T(8,128)(2,1)}, bf16[2,1024,2816]{2,1,0:T(8,128)(2,1)S(1)}, u32[]{:S(2)}) copy-start(bf16[2,1024,2816]{2,1,0:T(8,128)(2,1)S(1)} %convert.13) | copy-start | bytes 34603012
  37.1 110.1 %all-reduce.3.cloned.1.call-start = ((), (), s32[]{:S(2)}) async-start(), calls=%async_computation.6 | async-start | bytes 524288 | tf_op jit(solution)/shard_map/psum | solution.py:41
  37.2 26.5 %copy-start.3 = (f32[2,2816]{1,0:T(2,128)S(1)}, f32[2,2816]{1,0:T(2,128)}, u32[]{:S(2)}) copy-start(f32[2,2816]{1,0:T(2,128)} %param.14) | copy-start | bytes 67588
  37.2 26.5 %copy-start.4 = (f32[2,2816]{1,0:T(2,128)S(1)}, f32[2,2816]{1,0:T(2,128)}, u32[]{:S(2)}) copy-start(f32[2,2816]{1,0:T(2,128)} %param.13) | copy-start | bytes 67588
  49.8 66.1 %copy-start.5 = (f32[2,1024]{1,0:T(2,128)S(1)}, f32[2,1024]{1,0:T(2,128)}, u32[]{:S(2)}) copy-start(f32[2,1024]{1,0:T(2,128)} %param.15) | copy-start | bytes 24580
  115.8 71.0 %reduce-scatter.9.cloned.1.call-start = ((), (), s32[]{:S(2)}) async-start(), calls=%async_computation.7 | async-start | bytes 1802240 | tf_op jit(solution)/shard_map/reduce_scatter | solution.py:28
  153.1 68.1 %reduce-scatter.11.cloned.1.call-start = ((), (), s32[]{:S(2)}) async-start(), calls=%async_computation.8 | async-start | bytes 1802240 | tf_op jit(solution)/shard_map/reduce_scatter | solution.py:29
  157.8 130.5 %copy-start.6 = (f32[1024]{0:T(1024)S(1)}, f32[1024]{0:T(1024)}, u32[]{:S(2)}) copy-start(f32[1024]{0:T(1024)} %param.17) | copy-start | bytes 12292
  157.9 117.6 %all-reduce.5.cloned.1.call-start = ((), (), s32[]{:S(2)}) async-start(), calls=%async_computation.9 | async-start | bytes 524288 | tf_op jit(solution)/shard_map/psum | solution.py:41
Sparse Core Ops, SparseCore 0:
  22.3 36.0 reduce-scatter.4
  60.8 32.2 reduce-scatter.6
  116.0 31.2 all-reduce.2
  153.2 33.5 reduce-scatter.8
  189.0 32.1 reduce-scatter.10
  244.1 31.3 all-reduce.4
where the time goes:
time: 298 us; the launch traced here: 297 us
  waiting for transfers between devices  143 us (48%)
  blocking collectives  71.9 us (24%)
  other arithmetic  36.8 us (12%)
  matrix products  22 us (7%)
  between operations  13.6 us (5%)
  local copies, waits for them, and re-layouts  9.34 us (3%)
    reduce_scatter x2, waiting for transfers between devices, local(): lax.psum_scatter(operands[1], 'ra', scatter_dimension=0, tiled=True)  63.6 us
    psum x2, waiting for transfers between devices, local(): lax.psum(terms.astype(jnp.bfloat16), 'cb').astype(jnp.float32)  62.8 us
    all_gather x2, blocking collectives, local(): lax.all_gather(hidden, 'ra', axis=0, tiled=True)  34.3 us
    another operation x3, other arithmetic  29.8 us
    psum x2, blocking collectives, local(): total = lax.psum(squares, 'ra')  25.9 us
    reduce_scatter x2, waiting for transfers between devices, local(): lax.psum_scatter(operands[0], 'ra', scatter_dimension=0, tiled=True)  16.6 us
    psum x1, blocking collectives, local(): final_sum = lax.psum(jnp.sum(xvals * xvals, axis=1), 'ra')  11.7 us
    dot_general x2, matrix products, local(): jnp.dot(lax.all_gather(hidden, 'ra', axis=0, tiled=True), down_local, pre...  8.61 us
  transfers between devices with their start and end apart: 6, of which 5 were waited for; matrix products, arithmetic and copies ran while one was open for 10% of the time, Pallas kernels for 0%

commit v1 on v0

--- a/solution.py
+++ b/solution.py
@@ -5,6 +5,15 @@
 
 D = 4096
 LAYERS = 2
+
+
+def added_up(x, axis):
+    peers = lax.axis_size(axis)
+    result, far = (x, 1)
+    while far < peers:
+        result = result + lax.ppermute(result, axis, [(i, i ^ far) for i in range(peers)])
+        far = 2 * far
+    return result
 
 
 def local(stream, w_gate, w_up, w_down, gate_scale, up_scale, down_scale, pre_gain, out_gain):
@@ -22,7 +31,7 @@
             scaled, w_up[layer].astype(jnp.bfloat16), preferred_element_type=jnp.float32
         )
         down_local = w_down[layer].astype(jnp.bfloat16)
-        total = lax.psum(squares, "ra")
+        total = added_up(squares, "ra")
         operands = (gate_part, up_part)
         summed = (
             lax.psum_scatter(operands[0], "ra", scatter_dimension=0, tiled=True),

time: 298 us -> 297 us (level)
  blocking collectives: 71.9 us -> 46 us
  waiting for transfers between devices: 143 us -> 158 us
  starting transfers between devices: 0.21 us -> 10.5 us
    psum x2 -> x0, blocking collectives: 25.9 us -> none  [local(): total = lax.psum(squares, 'ra')]
    ppermute x0 -> x4, starting transfers between devices: none -> 10.3 us  [added_up(): lax.ppermute(result, axis, [(i, i ^ far) for i in range(peers)])]
    ppermute x0 -> x4, waiting for transfers between devices: none -> 6.06 us  [added_up(): lax.ppermute(result, axis, [(i, i ^ far) for i in range(peers)])]
    reduce_scatter x2, waiting for transfers between devices: 63.6 us -> 68.8 us  [local(): lax.psum_scatter(operands[1], 'ra', scatter_dimension=0, tiled=True)]
    reduce_scatter x2, waiting for transfers between devices: 16.6 us -> 20.7 us  [local(): lax.psum_scatter(operands[0], 'ra', scatter_dimension=0, tiled=True)]
  transfers between devices with their start and end apart: 6 -> 10, of which waited for: 5 -> 9; matrix products, arithmetic and copies ran while one was open for 10% -> 10% of each run, Pallas kernels for 0% -> 0%
where the time goes in v1:
time: 297 us
  waiting for transfers between devices  158 us (53%)
  blocking collectives  46 us (15%)
  other arithmetic  36.8 us (12%)
  matrix products  22 us (7%)
  between operations  13.6 us (5%)
  starting transfers between devices  10.5 us (4%)
  local copies, waits for them, and re-layouts  9.33 us (3%)
    reduce_scatter x2, waiting for transfers between devices, local(): lax.psum_scatter(operands[1], 'ra', scatter_dimension=0, tiled=True)  68.8 us
    psum x2, waiting for transfers between devices, local(): lax.psum(terms.astype(jnp.bfloat16), 'cb').astype(jnp.float32)  62.8 us
    all_gather x2, blocking collectives, local(): lax.all_gather(hidden, 'ra', axis=0, tiled=True)  34.3 us
    another operation x3, other arithmetic  29.8 us
    reduce_scatter x2, waiting for transfers between devices, local(): lax.psum_scatter(operands[0], 'ra', scatter_dimension=0, tiled=True)  20.7 us
    psum x1, blocking collectives, local(): final_sum = lax.psum(jnp.sum(xvals * xvals, axis=1), 'ra')  11.7 us
    ppermute x4, starting transfers between devices, added_up(): lax.ppermute(result, axis, [(i, i ^ far) for i in range(peers)])  10.3 us
    dot_general x2, matrix products, local(): jnp.dot(lax.all_gather(hidden, 'ra', axis=0, tiled=True), down_local, pre...  8.61 us
  transfers between devices with their start and end apart: 10, of which 9 were waited for; matrix products, arithmetic and copies ran while one was open for 10% of the time, Pallas kernels for 0%

profile of v1, /device:TPU:0, one launch (start us, length us, event | category | flops | bytes accessed | tf_op | source)
XLA Modules:
  0.0 296.7 jit_solution(12217988240336290537)
XLA Ops:
  6.5 0.8 fusion.24
  7.3 8.6 %convert.12 = bf16[2,1024,2816]{2,1,0:T(8,128)(2,1)S(1)} convert(f32[2,1024,2816]{2,1,0:T(8,128)} %param.10) | non-fusion elementwise | flops 5767168 | bytes 34603008 | tf_op jit(solution)/shard_map/convert.5
  15.9 4.2 %copy-done.1 = bf16[2,1024,2816]{2,1,0:T(8,128)(2,1)} copy-done((bf16[2,1024,2816]{2,1,0:T(8,128)(2,1)}, bf16[2,1024,2816]{2,1,0:T(8,128)(2,1)S(1)}, u32[]{:S(2)}) %copy-start.1) | copy-done | bytes 11534360
  20.1 2.0 fusion.5
  22.2 0.0 reduce-scatter.5.cloned.1.call-update
  22.2 0.0 reduce-scatter.7.cloned.1.call-start
  22.2 8.6 %convert.13 = bf16[2,1024,2816]{2,1,0:T(8,128)(2,1)S(1)} convert(f32[2,1024,2816]{2,1,0:T(8,128)} %param.11) | non-fusion elementwise | flops 5767168 | bytes 34603008 | tf_op jit(solution)/shard_map/convert.4
  30.8 4.2 %copy-done = bf16[2,1024,2816]{2,1,0:T(8,128)(2,1)} copy-done((bf16[2,1024,2816]{2,1,0:T(8,128)(2,1)}, bf16[2,1024,2816]{2,1,0:T(8,128)(2,1)S(1)}, u32[]{:S(2)}) %copy-start) | copy-done | bytes 11534360
  35.0 2.1 fusion.4
  37.1 0.0 reduce-scatter.7.cloned.1.call-update
  37.1 0.0 all-reduce.3.cloned.1.call-start
  37.2 0.1 fusion.14
  37.3 3.3 %collective-permute-start = (f32[128]{0:T(128)S(1)}, f32[128]{0:T(128)S(1)}, u32[]{:S(2)}, u32[]{:S(2)}) collective-permute-start(f32[128]{0:T(128)S(1)} %fusion.14), channel_id=1, source_target_pairs={{0,4},{4,0},{8,12},{12,8},{1,5},{5,1},{9,13},{13,9},{2,6},{6,2},{1... | collective-permute-start | bytes 1544 | tf_op jit(solution)/shard_map/ppermute | solution.py:14
  40.7 0.1 slice_reduce_fusion
  40.8 1.6 collective-permute-done
  42.4 3.0 collective-permute-start.1
  45.4 12.6 %convert.14 = bf16[2,2816,1024]{2,1,0:T(8,128)(2,1)} convert(f32[2,2816,1024]{2,1,0:T(8,128)} %param.12) | non-fusion elementwise | flops 5767168 | bytes 34603008 | tf_op jit(solution)/shard_map/convert.3
  58.0 0.1 add_rsqrt_fusion.2
  58.1 0.4 reduce-scatter.5.cloned.1.call-done
  58.5 34.5 %reduce-scatter.7.cloned.1.call-done = f32[32,2816]{1,0:T(8,128)} async-done(((f32[128,2816]{1,0:T(8,128)}), f32[32,2816]{1,0:T(8,128)}) %reduce-scatter.7.cloned.1.call-update) | async-done | bytes 360464 | tf_op jit(solution)/shard_map/reduce_scatter | solution.py:38
  93.0 1.3 multiply_convert_fusion.1
  94.3 17.2 %all_gather.6 = bf16[128,2816]{1,0:T(8,128)(2,1)S(1)} all-gather(bf16[32,2816]{1,0:T(8,128)(2,1)S(1)} %multiply_convert_fusion.1), channel_id=1, replica_groups=mesh['grp'=2,'ra'=4,'cb'=4] {'ra'}, dimensions={0}, use_global_device_ids=true | all-gather | bytes 901120 | tf_op jit(solution)/shard_map/all_gather | solution.py:46
  111.4 4.3 %fusion.6 = bf16[128,1024]{1,0:T(8,128)(2,1)} fusion(bf16[128,2816]{1,0:T(8,128)(2,1)S(1)} %all_gather.6, bf16[2,2816,1024]{2,1,0:T(8,128)(2,1)} %convert.14), kind=kOutput, calls=%fused_computation.12 | convolution fusion | flops 738328576 | bytes 6750208 | tf_op jit(solution)/shard_map/dot_general | solution.py:45
  115.8 0.0 all-reduce.3.cloned.1.call-update
  115.8 0.0 reduce-scatter.9.cloned.1.call-start
  115.9 31.3 %all-reduce.3.cloned.1.call-done = bf16[128,1024]{1,0:T(8,128)(2,1)} async-done(((bf16[128,1024]{1,0:T(8,128)(2,1)}), bf16[128,1024]{1,0:T(8,128)(2,1)}) %all-reduce.3.cloned.1.call-update) | async-done | bytes 262160 | tf_op jit(solution)/shard_map/psum | solution.py:50
  147.2 1.2 fusion.18
  148.3 4.7 %fusion.2 = f32[128,2816]{1,0:T(8,128)} fusion(bf16[2,1024,2816]{2,1,0:T(8,128)(2,1)} %copy-done.1, bf16[128,1024]{1,0:T(8,128)(2,1)S(1)} %get-tuple-element.10, f32[1024]{0:T(1024)S(1)} %bitcast.31), kind=kOutput, calls=%fused_computation.5 | convolution fusion | flops 738590720 | bytes 7475200 | tf_op jit(solution)/shard_map/dot_general | solution.py:27
  153.0 0.0 reduce-scatter.9.cloned.1.call-update
  153.0 0.0 reduce-scatter.11.cloned.1.call-start
  153.1 4.7 %fusion.1 = f32[128,2816]{1,0:T(8,128)} fusion(bf16[2,1024,2816]{2,1,0:T(8,128)(2,1)} %copy-done, bf16[128,1024]{1,0:T(8,128)(2,1)S(1)} %get-tuple-element.10, f32[1024]{0:T(1024)S(1)} %bitcast.32), kind=kOutput, calls=%fused_computation.3 | convolution fusion | flops 738590720 | bytes 7475200 | tf_op jit(solution)/shard_map/dot_general | solution.py:30
  157.8 0.0 reduce-scatter.11.cloned.1.call-update
  157.8 0.0 all-reduce.5.cloned.1.call-start
  157.8 1.6 collective-permute-start.2
  159.4 2.1 collective-permute-done.2
  161.5 2.4 collective-permute-start.3
  163.9 2.3 collective-permute-done.3
  166.2 0.1 add_rsqrt_fusion.1
  166.3 20.3 %reduce-scatter.9.cloned.1.call-done = f32[32,2816]{1,0:T(8,128)} async-done(((f32[128,2816]{1,0:T(8,128)}), f32[32,2816]{1,0:T(8,128)}) %reduce-scatter.9.cloned.1.call-update) | async-done | bytes 360464 | tf_op jit(solution)/shard_map/reduce_scatter | solution.py:37
  186.6 34.3 %reduce-scatter.11.cloned.1.call-done = f32[32,2816]{1,0:T(8,128)} async-done(((f32[128,2816]{1,0:T(8,128)}), f32[32,2816]{1,0:T(8,128)}) %reduce-scatter.11.cloned.1.call-update) | async-done | bytes 360464 | tf_op jit(solution)/shard_map/reduce_scatter | solution.py:38
  220.9 1.3 multiply_convert_fusion
  222.2 17.1 %all_gather.7 = bf16[128,2816]{1,0:T(8,128)(2,1)S(1)} all-gather(bf16[32,2816]{1,0:T(8,128)(2,1)S(1)} %multiply_convert_fusion), channel_id=1, replica_groups=mesh['grp'=2,'ra'=4,'cb'=4] {'ra'}, dimensions={0}, use_global_device_ids=true | all-gather | bytes 901120 | tf_op jit(solution)/shard_map/all_gather | solution.py:46
  239.4 4.3 %fusion.7 = bf16[128,1024]{1,0:T(8,128)(2,1)} fusion(bf16[128,2816]{1,0:T(8,128)(2,1)S(1)} %all_gather.7, bf16[2,2816,1024]{2,1,0:T(8,128)(2,1)} %convert.14), kind=kOutput, calls=%fused_computation.13 | convolution fusion | flops 738328576 | bytes 6750208 | tf_op jit(solution)/shard_map/dot_general | solution.py:45
  243.7 0.0 all-reduce.5.cloned.1.call-update
  243.7 31.5 %all-reduce.5.cloned.1.call-done = bf16[128,1024]{1,0:T(8,128)(2,1)} async-done(((bf16[128,1024]{1,0:T(8,128)(2,1)}), bf16[128,1024]{1,0:T(8,128)(2,1)}) %all-reduce.5.cloned.1.call-update) | async-done | bytes 262160 | tf_op jit(solution)/shard_map/psum | solution.py:50
  275.2 1.2 fusion.8
  276.3 11.7 %psum.23 = f32[128]{0:T(128)S(1)} all-reduce(f32[128]{0:T(128)S(1)} %fusion.8), channel_id=1, replica_groups=mesh['grp'=2,'ra'=4,'cb'=4] {'ra'}, use_global_device_ids=true, to_apply=%region_9.10 | all-reduce | flops 128 | bytes 1024 | tf_op jit(solution)/shard_map/psum | solution.py:53
  288.0 1.8 fusion.10
  (20 shorter events, 0.1 us)
Async XLA Ops:
  6.5 51.9 %reduce-scatter.5.cloned.1.call-start = ((), (), s32[]{:S(2)}) async-start(), calls=%async_computation.4 | async-start | bytes 1802240 | tf_op jit(solution)/shard_map/reduce_scatter | solution.py:37
  7.3 12.8 %copy-start.2 = (bf16[128,1024]{1,0:T(8,128)(2,1)S(1)}, bf16[128,1024]{1,0:T(8,128)(2,1)}, u32[]{:S(2)}) copy-start(bf16[128,1024]{1,0:T(8,128)(2,1)} %param.9) | copy-start | bytes 786436
  15.9 4.2 %copy-start.1 = (bf16[2,1024,2816]{2,1,0:T(8,128)(2,1)}, bf16[2,1024,2816]{2,1,0:T(8,128)(2,1)S(1)}, u32[]{:S(2)}) copy-start(bf16[2,1024,2816]{2,1,0:T(8,128)(2,1)S(1)} %convert.12) | copy-start | bytes 34603012
  22.2 70.8 %reduce-scatter.7.cloned.1.call-start = ((), (), s32[]{:S(2)}) async-start(), calls=%async_computation.5 | async-start | bytes 1802240 | tf_op jit(solution)/shard_map/reduce_scatter | solution.py:38
  30.8 4.2 %copy-start = (bf16[2,1024,2816]{2,1,0:T(8,128)(2,1)}, bf16[2,1024,2816]{2,1,0:T(8,128)(2,1)S(1)}, u32[]{:S(2)}) copy-start(bf16[2,1024,2816]{2,1,0:T(8,128)(2,1)S(1)} %convert.13) | copy-start | bytes 34603012
  35.0 5.6 %copy-start.3 = (f32[2,2816]{1,0:T(2,128)S(1)}, f32[2,2816]{1,0:T(2,128)}, u32[]{:S(2)}) copy-start(f32[2,2816]{1,0:T(2,128)} %param.14) | copy-start | bytes 67588
  35.0 5.6 %copy-start.4 = (f32[2,2816]{1,0:T(2,128)S(1)}, f32[2,2816]{1,0:T(2,128)}, u32[]{:S(2)}) copy-start(f32[2,2816]{1,0:T(2,128)} %param.13) | copy-start | bytes 67588
  37.1 110.1 %all-reduce.3.cloned.1.call-start = ((), (), s32[]{:S(2)}) async-start(), calls=%async_computation.6 | async-start | bytes 524288 | tf_op jit(solution)/shard_map/psum | solution.py:50
  37.3 5.1 %collective-permute-start = (f32[128]{0:T(128)S(1)}, f32[128]{0:T(128)S(1)}, u32[]{:S(2)}, u32[]{:S(2)}) collective-permute-start(f32[128]{0:T(128)S(1)} %fusion.14), channel_id=1, source_target_pairs={{0,4},{4,0},{8,12},{12,8},{1,5},{5,1},{9,13},{13,9},{2,6},{6,2},{1... | collective-permute-start | bytes 1544 | tf_op jit(solution)/shard_map/ppermute | solution.py:14
  42.4 15.6 %collective-permute-start.1 = (f32[128]{0:T(128)S(1)}, f32[128]{0:T(128)S(1)}, u32[]{:S(2)}, u32[]{:S(2)}) collective-permute-start(f32[128]{0:T(128)S(1)} %add.55), channel_id=1, source_target_pairs={{0,8},{4,12},{8,0},{12,4},{1,9},{5,13},{9,1},{13,5},{2,10},{6,14},... | collective-permute-start | bytes 1544 | tf_op jit(solution)/shard_map/ppermute | solution.py:14
  58.0 57.8 %copy-start.5 = (f32[2,1024]{1,0:T(2,128)S(1)}, f32[2,1024]{1,0:T(2,128)}, u32[]{:S(2)}) copy-start(f32[2,1024]{1,0:T(2,128)} %param.15) | copy-start | bytes 24580
  115.8 70.8 %reduce-scatter.9.cloned.1.call-start = ((), (), s32[]{:S(2)}) async-start(), calls=%async_computation.7 | async-start | bytes 1802240 | tf_op jit(solution)/shard_map/reduce_scatter | solution.py:37
  153.0 67.9 %reduce-scatter.11.cloned.1.call-start = ((), (), s32[]{:S(2)}) async-start(), calls=%async_computation.8 | async-start | bytes 1802240 | tf_op jit(solution)/shard_map/reduce_scatter | solution.py:38
  157.8 130.3 %copy-start.6 = (f32[1024]{0:T(1024)S(1)}, f32[1024]{0:T(1024)}, u32[]{:S(2)}) copy-start(f32[1024]{0:T(1024)} %param.17) | copy-start | bytes 12292
  157.8 117.4 %all-reduce.5.cloned.1.call-start = ((), (), s32[]{:S(2)}) async-start(), calls=%async_computation.9 | async-start | bytes 524288 | tf_op jit(solution)/shard_map/psum | solution.py:50
  157.8 3.6 %collective-permute-start.2 = (f32[128]{0:T(128)S(1)}, f32[128]{0:T(128)S(1)}, u32[]{:S(2)}, u32[]{:S(2)}) collective-permute-start(f32[128]{0:T(128)S(1)} %get-tuple-element.9), channel_id=1, source_target_pairs={{0,4},{4,0},{8,12},{12,8},{1,5},{5,1},{9,13},{13,9},{2,6},{6,2},{1... | collective-permute-start | bytes 1544 | tf_op jit(solution)/shard_map/ppermute | solution.py:14
  161.5 4.7 %collective-permute-start.3 = (f32[128]{0:T(128)S(1)}, f32[128]{0:T(128)S(1)}, u32[]{:S(2)}, u32[]{:S(2)}) collective-permute-start(f32[128]{0:T(128)S(1)} %add.61), channel_id=1, source_target_pairs={{0,8},{4,12},{8,0},{12,4},{1,9},{5,13},{9,1},{13,5},{2,10},{6,14},... | collective-permute-start | bytes 1544 | tf_op jit(solution)/shard_map/ppermute | solution.py:14
Sparse Core Ops, SparseCore 0:
  22.3 36.1 reduce-scatter.4
  60.8 32.1 reduce-scatter.6
  115.9 31.2 all-reduce.2
  153.1 33.4 reduce-scatter.8
  188.8 32.1 reduce-scatter.10
  243.8 31.3 all-reduce.4
